TPU v7x, 32 devices: a whole 2x2x4 slice. The times are simulated.
32 devices in a mesh: grp: 2 (over y), sp: 4 (over z), tp: 4 (over x, core).
Axes of the slice: x: 2, y: 2, z: 4, core: 2. Of those that a mesh axis runs over, the one named last changes fastest.
Arguments:
- tokens: bfloat16 [1024, 2048], P(('grp', 'sp'), 'tp'), parts along dimension 0, may hold values from -6 to 6
- norm_gain: float32 [2048], replicated, may hold values from 0.1 to 1.9
- att_q_weight: bfloat16 [1024, 2048], P('tp', 'sp'), may hold values from -0.625 to 0.625
- att_k_weight: bfloat16 [512, 2048], P('tp', 'sp'), may hold values from -0.125 to 0.125
- att_v_weight: bfloat16 [512, 2048], P('tp', 'sp'), may hold values from -0.125 to 0.125
- rec_q_weight: bfloat16 [1024, 2048], P('tp', 'sp'), may hold values from -0.125 to 0.125
- rec_f_weight: bfloat16 [1024, 2048], P('tp', 'sp'), may hold values from -0.125 to 0.125
- rec_i_weight: bfloat16 [1024, 2048], P('tp', 'sp'), may hold values from -0.125 to 0.125
- att_out_weight: bfloat16 [1024, 2048], P('tp', 'sp'), may hold values from -1.5 to 1.5
- rec_out_weight: bfloat16 [1024, 2048], P('tp', 'sp'), may hold values from -0.1875 to 0.1875
- score_offset: float32 [16], P('tp'), may hold values from -11.5 to -3
- lower_bound: float32 [1024], P('tp'), may hold values from 0.94 to 0.99999
- decay_shift: float32 [1024, 1024], P(('grp', 'sp'), 'tp'), parts along dimension 0, may hold values from -2.1 to 0
- rec_gain: float32 [1024], P('tp'), may hold values from 0.1 to 1.9
Outputs:
- mixed: bfloat16 [1024, 2048], P(('grp', 'sp', 'tp')), parts along dimension 0
There are 2 independent parts, one for each index of `grp`. A program takes and returns all parts, laid end to end along the dimension named above; an argument that names none is the same for every part. Nothing has to cross between parts.
All inputs are finite; a program needn't handle non-finite values.
Results may differ from a plain program's by a relative error of at most 0.015.
Values may be sent and summed in bfloat16 or wider, within the bound.
A program may use at most 64 MiB of HBM per device.

v0:
```python
import jax
import jax.numpy as jnp
from jax import lax
from jax.sharding import PartitionSpec as P

HEAD = 64
REC_KEY = 128
REC_VAL = 128
SPAN = 64


EPS = 1e-06
TOP_PRECISION = lax.Precision.HIGHEST


def entering(x, axis, combine, identity):
    count, here = (lax.axis_size(axis), lax.axis_index(axis))
    everything = jax.tree.map(
        lambda part, kind: lax.all_gather(part.astype(kind), axis), x, (jnp.bfloat16, jnp.bfloat16)
    )
    start = jax.tree.map(
        lambda part, zero: jnp.broadcast_to(jnp.asarray(zero, part.dtype), part.shape), x, identity
    )

    def entering_turn(k, before):
        reached = k < here
        new = combine(
            before, jax.tree.map(lambda part, own: part[k].astype(own.dtype), everything, x)
        )
        return jax.tree.map(lambda a, b: jnp.where(reached, a, b), new, before)

    return lax.fori_loop(0, count, entering_turn, start)


def make_fold(norm_gain, weights, carry, piece):
    elementwise_sq, totals = carry
    raw = piece.astype(jnp.float32)
    scaled = (raw * norm_gain[None, :]).astype(jnp.bfloat16)
    elementwise_sq = jnp.sum(raw * raw, axis=1)
    updated = []
    for total, weight in zip(totals, weights):
        updated.append(
            lax.dot_general(
                scaled, weight, (((1,), (1,)), ((), ())), preferred_element_type=jnp.float32
            )
        )
    return (elementwise_sq, tuple(updated))


def project_all(tokens, norm_gain, weights):
    rows = tokens.shape[0]
    width = weights[0].shape[1]
    start_carry = (
        jnp.zeros((rows,), jnp.float32),
        tuple((jnp.zeros((rows, weight.shape[0]), jnp.float32) for weight in weights)),
    )
    elementwise_sq, totals = make_fold(
        norm_gain, weights, start_carry, lax.all_gather(tokens, "tp", axis=1, tiled=True)
    )
    inv_rms = lax.rsqrt(elementwise_sq / width + EPS)
    return tuple((total * inv_rms[:, None] for total in totals))


def attention(att_query, key_value, score_offset):
    rows = att_query.shape[0]
    gathered = lax.all_gather(key_value, "sp", axis=0, tiled=True)
    seq = gathered.shape[0]
    kv_heads = key_value.shape[1] // (2 * HEAD)
    q_heads = att_query.shape[1] // HEAD
    group = q_heads // kv_heads
    kv_width = kv_heads * HEAD
    queries = att_query.reshape(rows, kv_heads, group, HEAD)
    offsets = score_offset.reshape(kv_heads, group)
    kblock = min(1024, seq)
    first_row = lax.axis_index("sp") * rows
    query_pos = first_row + jnp.arange(rows, dtype=jnp.int32)
    count = (first_row + rows - 1) // kblock + 1

    def attention_turn(step, carry):
        summed, run = carry
        block_start = (count - 1 - step) * kblock
        block = lax.dynamic_slice_in_dim(gathered, block_start, kblock, 0)
        keys = block[:, :kv_width].reshape(kblock, kv_heads, HEAD)
        values = block[:, kv_width:].reshape(kblock, kv_heads, HEAD)
        score = (
            jnp.einsum("tkgd,skd->tkgs", queries, keys, preferred_element_type=jnp.float32)
            * HEAD ** (-0.5)
            + offsets[None, :, :, None]
        )
        key_pos = block_start + jnp.arange(kblock, dtype=jnp.int32)
        visible = (key_pos[None, :] < query_pos[:, None])[:, None, None, :]
        keep = jnp.where(visible, jax.nn.log_sigmoid(-score), 0.0)
        tail = lax.cumsum(keep, axis=3, reverse=True) - keep
        weight = jnp.where(
            visible, jnp.exp(jax.nn.log_sigmoid(score) + tail + run[..., None]), 0.0
        ).astype(jnp.bfloat16)
        summed = summed + jnp.einsum(
            "tkgs,skd->tkgd", weight, values, preferred_element_type=jnp.float32
        )
        return (summed, run + jnp.sum(keep, axis=3))

    start_carry = (
        jnp.zeros((rows, kv_heads, group, HEAD), jnp.float32),
        jnp.zeros((rows, kv_heads, group), jnp.float32),
    )
    summed, _ = lax.fori_loop(0, count, attention_turn, start_carry)
    return summed.reshape(rows, q_heads * HEAD).astype(jnp.bfloat16)


def block_pass(carry, inputs):
    state_matrix, prefix = carry
    query_rows, log_decay, keyed_values, value_rows = inputs
    span = query_rows.shape[0]
    cumulative_log = jnp.cumsum(log_decay, axis=0)
    lower = jnp.arange(span, dtype=jnp.int32)[:, None] >= jnp.arange(span, dtype=jnp.int32)[None, :]
    diff = cumulative_log[:, None] - cumulative_log[None, :]
    decay = jnp.exp(jnp.where(lower[:, :, None, None], diff, -jnp.inf))
    score = jnp.einsum(
        "thk,tshk,shk->ths", query_rows, decay, keyed_values, precision=TOP_PRECISION
    )
    inner = jnp.einsum("ths,shv->thv", score, value_rows, precision=TOP_PRECISION)
    outer_product = jnp.einsum(
        "ril,ilc->ric", query_rows * jnp.exp(cumulative_log), state_matrix, precision=TOP_PRECISION
    )
    final_state = cumulative_log[-1]
    state_matrix = state_matrix * jnp.exp(final_state)[:, :, None] + jnp.einsum(
        "iag,iax->agx",
        keyed_values * jnp.exp(final_state[None] - cumulative_log),
        value_rows,
        precision=TOP_PRECISION,
    )
    reach_limit = query_rows * jnp.exp(cumulative_log + prefix[None])
    return ((state_matrix, prefix + final_state), (inner + outer_product, reach_limit))


def chain(earlier, later):
    return (earlier[0] * later[0], earlier[1] * later[0][:, :, None] + later[1])


def recurrence(rec_query, rec_forget, rec_input, lower_bound, decay_shift, rec_gain):
    rows = rec_query.shape[0]
    heads = rec_gain.shape[0] // REC_VAL
    logit = rec_forget.astype(jnp.float32)
    gap = 1.0 - lower_bound
    log_decay = jnp.log(lower_bound + gap * jax.nn.sigmoid(logit)) + decay_shift
    keyed_values = gap * jax.nn.sigmoid(-logit)
    query_rows = jax.nn.silu(rec_query.astype(jnp.float32))
    blocks = rows // SPAN

    def split(array, depth):
        return array.reshape(blocks, SPAN, heads, depth)

    start_carry = (
        jnp.zeros((heads, REC_KEY, REC_VAL), jnp.float32),
        jnp.zeros((heads, REC_KEY), jnp.float32),
    )
    (state_matrix, total), (local, reach_limit) = lax.scan(
        block_pass,
        start_carry,
        (
            split(query_rows, REC_KEY),
            split(log_decay, REC_KEY),
            split(keyed_values, REC_KEY),
            split(rec_input.astype(jnp.float32), REC_VAL),
        ),
    )
    identity = (
        jnp.ones((heads, REC_KEY), jnp.float32),
        jnp.zeros((heads, REC_KEY, REC_VAL), jnp.float32),
    )
    incoming_state = entering((jnp.exp(total), state_matrix), "sp", chain, identity)
    running_memory = jnp.einsum(
        "lida,dao->lido", reach_limit, incoming_state[1], precision=TOP_PRECISION
    )
    rec_raw = (local + running_memory).reshape(rows, heads, REC_VAL)
    rescaled_input = (
        rec_raw
        * lax.rsqrt(jnp.mean(rec_raw * rec_raw, axis=2, keepdims=True) + EPS)
        * rec_gain.reshape(heads, REC_VAL)
    )
    return rescaled_input.reshape(rows, heads * REC_VAL).astype(jnp.bfloat16)


def on_device(
    tokens,
    norm_gain,
    att_q_weight,
    att_k_weight,
    att_v_weight,
    rec_q_weight,
    rec_f_weight,
    rec_i_weight,
    att_out_weight,
    rec_out_weight,
    score_offset,
    lower_bound,
    decay_shift,
    rec_gain,
):
    inputs = (
        lax.all_gather(att_q_weight, "sp", axis=1, tiled=True),
        lax.all_gather(att_k_weight, "sp", axis=1, tiled=True),
        lax.all_gather(att_v_weight, "sp", axis=1, tiled=True),
        lax.all_gather(rec_q_weight, "sp", axis=1, tiled=True),
        lax.all_gather(rec_f_weight, "sp", axis=1, tiled=True),
        lax.all_gather(rec_i_weight, "sp", axis=1, tiled=True),
    )
    projected = project_all(tokens, norm_gain, inputs)
    att_query = projected[0].astype(jnp.bfloat16)
    key_value = jnp.concatenate(projected[1:3], axis=1).astype(jnp.bfloat16)
    rec_query = projected[3].astype(jnp.bfloat16)
    rec_forget = projected[4].astype(jnp.bfloat16)
    rec_input = projected[5].astype(jnp.bfloat16)
    att_out = attention(att_query, key_value, score_offset)
    rec_out = recurrence(rec_query, rec_forget, rec_input, lower_bound, decay_shift, rec_gain)
    outputs = (
        lax.all_gather(att_out_weight, "sp", axis=1, tiled=True),
        lax.all_gather(rec_out_weight, "sp", axis=1, tiled=True),
    )
    att_rows, rec_rows = outputs
    return lax.psum_scatter(
        (
            jnp.dot(att_out, att_rows, preferred_element_type=jnp.float32)
            + jnp.dot(rec_out, rec_rows, preferred_element_type=jnp.float32)
        ).astype(jnp.bfloat16),
        "tp",
        scatter_dimension=0,
        tiled=True,
    )


def solution(mesh):
    in_specs = (
        P(("grp", "sp"), "tp"),
        P(),
        P("tp", "sp"),
        P("tp", "sp"),
        P("tp", "sp"),
        P("tp", "sp"),
        P("tp", "sp"),
        P("tp", "sp"),
        P("tp", "sp"),
        P("tp", "sp"),
        P("tp"),
        P("tp"),
        P(("grp", "sp"), "tp"),
        P("tp"),
    )
    out_specs = P(("grp", "sp", "tp"), None)
    return jax.shard_map(
        on_device, mesh=mesh, in_specs=in_specs, out_specs=out_specs, check_vma=False
    )
```

profile of v0, /device:TPU:0, one launch (start us, length us, event | category | flops | bytes accessed | tf_op | source)
XLA Modules:
  0.0 229.1 jit_solution(16450869114804737133)
XLA Ops:
  6.5 0.7 all-gather.14.cloned.1.call-update
  7.3 0.7 all-gather.18.cloned.1.call-update
  8.1 0.7 all-gather.16.cloned.1.call-update
  9.4 0.5 all-gather.12.cloned.1.call-update
  10.6 8.9 %all_gather.42 = bf16[128,2048]{1,0:T(8,128)(2,1)S(1)} all-gather(bf16[128,512]{1,0:T(8,128)(2,1)} %param.20), channel_id=1, replica_groups=mesh['grp'=2,'sp'=4,'tp'=4] {'tp'}, dimensions={1}, use_global_device_ids=true | all-gather | bytes 655360 | tf_op jit(solution)/shard_map/all_gather | solution.py:58
  19.6 0.7 broadcast_subtract_fusion
  20.3 23.2 %all_gather.43 = bf16[128,2048]{1,0:T(8,128)(2,1)S(1)} all-gather(bf16[128,512]{1,0:T(8,128)(2,1)} %param.23), channel_id=1, replica_groups=mesh['grp'=2,'sp'=4,'tp'=4] {'sp'}, dimensions={1}, use_global_device_ids=true | all-gather | bytes 655360 | tf_op jit(solution)/shard_map/all_gather | solution.py:202
  43.6 16.3 %all_gather.44 = bf16[128,2048]{1,0:T(8,128)(2,1)S(1)} all-gather(bf16[128,512]{1,0:T(8,128)(2,1)} %param.24), channel_id=1, replica_groups=mesh['grp'=2,'sp'=4,'tp'=4] {'sp'}, dimensions={1}, use_global_device_ids=true | all-gather | bytes 655360 | tf_op jit(solution)/shard_map/all_gather | solution.py:203
  59.9 1.0 fusion.46
  61.3 18.9 %all_gather.45 = bf16[512,256]{0,1:T(8,128)(2,1)S(1)} all-gather(bf16[128,256]{0,1:T(8,128)(2,1)S(1)} %pad_maximum_fusion), channel_id=1, replica_groups=mesh['grp'=2,'sp'=4,'tp'=4] {'sp'}, dimensions={0}, use_global_device_ids=true | all-gather | bytes 327680 | tf_op jit(solution)/shard_map/all_gather | solution.py:66
  80.2 1.8 divide_multiply_fusion.1
  82.2 1.7 divide_multiply_fusion
  84.0 27.1 %all-gather.16.cloned.1.call-done = bf16[256,2048]{1,0:T(8,128)(2,1)} async-done(((bf16[256,512]{1,0:T(8,128)(2,1)}), bf16[256,2048]{1,0:T(8,128)(2,1)}) %all-gather.16.cloned.1.call-update) | async-done | bytes 1048592 | tf_op jit(solution)/shard_map/all_gather | solution.py:206
  111.1 1.7 fusion.43
  112.9 27.5 %while.47 = (s32[]{:T(128)}, f32[2,128,128]{2,1,0:T(8,128)S(1)}, f32[2,128]{1,0:T(2,128)S(1)}, f32[2,64,2,128]{3,1,0,2:T(8,128)S(1)}, f32[2,64,2,128]{3,1,0,2:T(...) while((s32[]{:T(128)}, f32[2,128,128]{2,1,0:T(8,128)S(1)}, ...), condition=%wide.region_8.9_spmd.clone, body=%wide.region_6.8_spmd.clone.sunk | while | flops 79909376 | bytes 10569869 | solution.py:157
  113.2 5.9 %multiply_bitcast_fusion.2 = f32[64,2,128,64]{2,1,0,3:T(2,128)S(1)} fusion(pred[64,64]{1,0:T(8,128)(4,1)S(1)} %iota_compare_fusion.2, f32[64,2,128]{2,1,0:T(2,128)S(1)} %get-tuple-element.589, f32[64,2,128]{2,1,0:T(2,128)S(1)} %fusion.122), kind=kLoop, calls=%fused_computation.27.clone.1 | loop fusion | flops 3145728 | bytes 4329472 | tf_op jit(solution)/shard_map/while/body/eval_jaxpr/thk,tshk,shk->ths/dot_general | solution.py:118
  119.2 6.6 %fusion.125 = f32[64,2,1,64]{3,2,1,0:T(1,128)S(1)} fusion(f32[64,2,128,1]{2,3,1,0:T(1,128)S(1)} %bitcast.180, f32[64,2,128,64]{2,1,0,3:T(2,128)S(1)} %multiply_bitcast_fusion.2), kind=kOutput, calls=%fused_computation.25.clone.1 | convolution fusion | flops 12582912 | bytes 4292608 | tf_op jit(solution)/shard_map/while/body/eval_jaxpr/thk,tshk,shk->ths/dot_general | solution.py:118
  127.0 5.9 %multiply_bitcast_fusion.2 = f32[64,2,128,64]{2,1,0,3:T(2,128)S(1)} fusion(pred[64,64]{1,0:T(8,128)(4,1)S(1)} %iota_compare_fusion.2, f32[64,2,128]{2,1,0:T(2,128)S(1)} %get-tuple-element.589, f32[64,2,128]{2,1,0:T(2,128)S(1)} %fusion.122), kind=kLoop, calls=%fused_computation.27.clone.1 | loop fusion | flops 3145728 | bytes 4329472 | tf_op jit(solution)/shard_map/while/body/eval_jaxpr/thk,tshk,shk->ths/dot_general | solution.py:118
  132.9 6.6 %fusion.125 = f32[64,2,1,64]{3,2,1,0:T(1,128)S(1)} fusion(f32[64,2,128,1]{2,3,1,0:T(1,128)S(1)} %bitcast.180, f32[64,2,128,64]{2,1,0,3:T(2,128)S(1)} %multiply_bitcast_fusion.2), kind=kOutput, calls=%fused_computation.25.clone.1 | convolution fusion | flops 12582912 | bytes 4292608 | tf_op jit(solution)/shard_map/while/body/eval_jaxpr/thk,tshk,shk->ths/dot_general | solution.py:118
  140.5 14.9 %all-gather.1 = bf16[8,128,128]{2,1,0:T(8,128)(2,1)S(1)} all-gather(bf16[2,128,128]{2,1,0:T(8,128)(2,1)S(1)} %convert_element_type.84), channel_id=3, replica_groups=mesh['grp'=2,'sp'=4,'tp'=4] {'sp'}, dimensions={0}, use_global_device_ids=true | all-gather | bytes 327680 | tf_op jit(solution)/shard_map/all_gather | solution.py:19
  155.4 10.2 %all-gather.2 = bf16[4,2,128]{2,1,0:T(2,128)(2,1)S(1)} all-gather(bf16[1,2,128]{2,1,0:T(2,128)(2,1)S(1)} %fusion.62), channel_id=2, replica_groups=mesh['grp'=2,'sp'=4,'tp'=4] {'sp'}, dimensions={0}, use_global_device_ids=true | all-gather | bytes 2560 | tf_op jit(solution)/shard_map/all_gather | solution.py:19
  165.7 1.7 fusion.39
  167.6 9.5 %while.46 = (s32[]{:T(128)}, f32[128,2,2,64]{0,3,2,1:T(8,128)S(1)}, f32[128,2,2]{0,2,1:T(2,128)S(1)}, s32[]{:T(128)}, s32[]{:T(128)}, /*index=5*/bf16[512,256]{0...) while((s32[]{:T(128)}, f32[128,2,2,64]{0,3,2,1:T(8,128)S(1)}, ...), condition=%wide.region_5.6_spmd.clone, body=%wide.region_1.5_spmd.clone.sunk | while | flops 109158528 | bytes 12920009 | solution.py:106
  168.0 1.0 fusion.111
  169.0 5.9 %fusion.112 = f32[128,2,2,4,128]{0,3,2,1,4:T(4,128)S(1)} fusion(f32[128,2,2,4,128]{0,4,3,2,1:T(8,128)S(1)} %bitcast.179), kind=kOutput, calls=%fused_computation.17.clone.1 | output fusion | flops 33292288 | bytes 2097152 | tf_op jit(solution)/shard_map/reduce-window.4
  175.4 1.5 fusion.113
  177.1 0.7 while.48
  177.8 1.2 fusion.65
  179.4 1.6 fusion.64
  181.0 17.5 %all-gather.20.cloned.1.call-done = bf16[256,2048]{1,0:T(8,128)(2,1)} async-done(((bf16[256,512]{1,0:T(8,128)(2,1)}), bf16[256,2048]{1,0:T(8,128)(2,1)}) %all-gather.20.cloned.1.call-update) | async-done | bytes 1048592 | tf_op jit(solution)/shard_map/all_gather | solution.py:218
  198.6 2.4 %fusion.38 = bf16[128,2048]{1,0:T(8,128)(2,1)} fusion(f32[128,2048]{1,0:T(8,128)S(1)} %fusion.64, bf16[256,2048]{1,0:T(8,128)(2,1)} %all-gather.20.cloned.1.call-done, f32[16,8,2,128]{3,2,1,0:T(2,128)S(1)} %bitcast.187, f32[16,8,2,128]{3,2,1,0:T(2,128)S(1)} %bitcast.186, f32[256]{0:T(256)S(1)} %copy-done.2), kind=kOutput, calls=%fused_computation.65 | convolution fusion | flops 134840320 | bytes 2884608 | tf_op jit(solution)/shard_map/dot_general | solution.py:224
  201.0 21.2 %reduce-scatter.2.cloned.1.call-done = bf16[32,2048]{1,0:T(8,128)(2,1)} async-done(((bf16[128,2048]{1,0:T(8,128)(2,1)}), bf16[32,2048]{1,0:T(8,128)(2,1)}) %reduce-scatter.2.cloned.1.call-update) | async-done | bytes 131088 | tf_op jit(solution)/shard_map/reduce_scatter | solution.py:221
  (90 shorter events, 6.6 us)
Async XLA Ops:
  6.5 73.7 %copy-start.3 = (f32[256]{0:T(256)S(1)}, f32[256]{0:T(256)}, u32[]{:S(2)}) copy-start(f32[256]{0:T(256)} %param.31) | copy-start | bytes 3076
  6.5 54.4 %copy-start.1 = (f32[2048]{0:T(1024)S(1)}, f32[2048]{0:T(1024)}, u32[]{:S(2)}) copy-start(f32[2048]{0:T(1024)} %param.21) | copy-start | bytes 24580
  6.5 73.7 %copy-start.4 = (f32[128,256]{1,0:T(8,128)S(1)}, f32[128,256]{1,0:T(8,128)}, u32[]{:S(2)}) copy-start(f32[128,256]{1,0:T(8,128)} %param.32) | copy-start | bytes 393220
  6.5 73.7 %all-gather.14.cloned.1.call-start = ((), (), s32[]{:S(2)}) async-start(), calls=%async_computation.3 | async-start | bytes 1310720 | tf_op jit(solution)/shard_map/all_gather | solution.py:205
  7.3 74.9 %all-gather.18.cloned.1.call-start = ((), (), s32[]{:S(2)}) async-start(), calls=%async_computation.5 | async-start | bytes 1310720 | tf_op jit(solution)/shard_map/all_gather | solution.py:204
  8.0 103.1 %all-gather.16.cloned.1.call-start = ((), (), s32[]{:S(2)}) async-start(), calls=%async_computation.4 | async-start | bytes 1310720 | tf_op jit(solution)/shard_map/all_gather | solution.py:206
  8.7 156.9 %all-gather.10.cloned.1.call-start = ((), (), s32[]{:S(2)}) async-start(), calls=%async_computation.1 | async-start | bytes 1310720 | tf_op jit(solution)/shard_map/all_gather | solution.py:201
  9.3 170.1 %all-gather.12.cloned.1.call-start = ((), (), s32[]{:S(2)}) async-start(), calls=%async_computation.2 | async-start | bytes 1310720 | tf_op jit(solution)/shard_map/all_gather | solution.py:217
  9.9 188.5 %all-gather.20.cloned.1.call-start = ((), (), s32[]{:S(2)}) async-start(), calls=%async_computation.6 | async-start | bytes 1310720 | tf_op jit(solution)/shard_map/all_gather | solution.py:218
  10.5 211.7 %reduce-scatter.2.cloned.1.call-start = ((), (), s32[]{:S(2)}) async-start(), calls=%async_computation.7 | async-start | bytes 655360 | tf_op jit(solution)/shard_map/reduce_scatter | solution.py:221
  112.9 54.6 %copy-start.5 = (f32[4]{0:T(128)S(1)}, f32[4]{0:T(128)}, u32[]{:S(2)}) copy-start(f32[4]{0:T(128)} %param.30) | copy-start | bytes 52
  140.4 27.1 %copy-start = (f32[2,64,2,128]{3,1,0,2:T(8,128)}, f32[2,64,2,128]{3,1,0,2:T(8,128)S(1)}, u32[]{:S(2)}) copy-start(f32[2,64,2,128]{3,1,0,2:T(8,128)S(1)} %get-tuple-element.256) | copy-start | bytes 393220
  177.1 21.5 %copy-start.2 = (f32[256]{0:T(256)S(1)}, f32[256]{0:T(256)}, u32[]{:S(2)}) copy-start(f32[256]{0:T(256)} %param.33) | copy-start | bytes 3076
Sparse Core Ops, SparseCore 0:
  8.9 39.1 all-gather.13
  49.6 32.2 all-gather.17
  83.5 27.5 all-gather.15
  112.5 27.4 all-gather.9
  141.4 28.0 all-gather.11
  171.0 27.4 all-gather.19
  201.1 21.0 reduce-scatter.1
where the time goes:
time: 230 us; the launch traced here: 229 us
  blocking collectives  92.5 us (40%)
  waiting for transfers between devices  69.5 us (30%)
  matrix products  29.5 us (13%)
  other arithmetic  21.6 us (9%)
  between operations  13.8 us (6%)
    all_gather x1, waiting for transfers between devices, on_device(): lax.all_gather(rec_i_weight, 'sp', axis=1, tiled=True)  27.1 us
    all_gather x2, blocking collectives, entering(): lax.all_gather(part.astype(kind), axis)  25.2 us
    all_gather x1, blocking collectives, on_device(): lax.all_gather(att_k_weight, 'sp', axis=1, tiled=True)  23.2 us
    reduce_scatter x1, waiting for transfers between devices, on_device(): lax.psum_scatter((jnp.dot(att_out, att_rows, preferred_element_type=jnp.f...  21.2 us
    all_gather x1, blocking collectives, attention(): gathered = lax.all_gather(key_value, 'sp', axis=0, tiled=True)  18.9 us
    all_gather x1, waiting for transfers between devices, on_device(): lax.all_gather(rec_out_weight, 'sp', axis=1, tiled=True)  17.5 us
    all_gather x1, blocking collectives, on_device(): lax.all_gather(att_v_weight, 'sp', axis=1, tiled=True)  16.3 us
    dot_general x2, matrix products, block_pass(): jnp.einsum('thk,tshk,shk->ths', query_rows, decay, keyed_values, precisio...  13.3 us
  transfers between devices with their start and end apart: 7, of which 3 were waited for; matrix products, arithmetic and copies ran while one was open for 22% of the time, Pallas kernels for 0%

commit v1 on v0

--- a/solution.py
+++ b/solution.py
@@ -1,6 +1,10 @@
+import functools
+
 import jax
 import jax.numpy as jnp
 from jax import lax
+from jax.experimental import pallas as pl
+from jax.experimental.pallas import tpu as pltpu
 from jax.sharding import PartitionSpec as P
 
 HEAD = 64
@@ -181,7 +185,7 @@
     return rescaled_input.reshape(rows, heads * REC_VAL).astype(jnp.bfloat16)
 
 
-def on_device(
+def gathered_plan(
     tokens,
     norm_gain,
     att_q_weight,
@@ -229,6 +233,540 @@
     )
 
 
+MESH = pl.DeviceIdType.MESH
+HALVES = 2
+STEP = 32
+
+
+def dot_nt(a, b):
+    return lax.dot_general(a, b, (((1,), (1,)), ((), ())), preferred_element_type=jnp.float32)
+
+
+def dot_tn(a, b):
+    return lax.dot_general(a, b, (((0,), (0,)), ((), ())), preferred_element_type=jnp.float32)
+
+
+def dot_nn(a, b):
+    return jnp.dot(a, b, preferred_element_type=jnp.float32)
+
+
+def remote(src, dst, send_sem, recv_sem, target):
+    return pltpu.make_async_remote_copy(
+        src_ref=src,
+        dst_ref=dst,
+        send_sem=send_sem,
+        recv_sem=recv_sem,
+        device_id=target,
+        device_id_type=MESH,
+    )
+
+
+def role_table(count, att_count, rec_count):
+    first = rec_count - rec_count // 2
+    return (
+        [("rec", j) for j in range(first)]
+        + [("att", j) for j in range(att_count)]
+        + [("rec", j) for j in range(first, rec_count)]
+    )
+
+
+def select_static(index, values):
+    result = jnp.int32(0)
+    for k, value in enumerate(values):
+        result = jnp.where(index == k, jnp.int32(value), result)
+    return result
+
+
+def project_kernel(
+    roles, n, nt, width,
+    tok_ref, gain_ref, aq_ref, ak_ref, av_ref, rq_ref, rf_ref, ri_ref, shift_ref,
+    out_ref, shifts_ref,
+    tbuf, squares, scaled, part, send_r, recv_r, send_l, recv_l,
+    a_send, a_recv, a_local, b_send, b_recv, d_send, d_recv, d_local, q_send, q_recv,
+    rs_sem, rr_sem, ls_sem, lr_sem,
+):
+    s, t = lax.axis_index("sp"), lax.axis_index("tp")
+    rows, feats = tok_ref.shape
+    piece = rows // nt
+    seq = rows * n
+
+    barrier = pltpu.get_barrier_semaphore()
+    for a in range(n):
+        for b in range(nt):
+            if a or b:
+                pl.semaphore_signal(
+                    barrier, inc=1,
+                    device_id={"sp": lax.rem(s + a, n), "tp": lax.rem(t + b, nt)},
+                    device_id_type=MESH,
+                )
+    pl.semaphore_wait(barrier, n * nt - 1)
+
+    def first_copy(j):
+        return remote(
+            tok_ref.at[pl.ds(j * piece, piece)], tbuf.at[s, j], a_send.at[j], a_recv.at[s],
+            {"sp": t, "tp": j},
+        )
+
+    def first_here(j):
+        return pltpu.make_async_copy(
+            tok_ref.at[pl.ds(j * piece, piece)], tbuf.at[s, j], a_local
+        )
+
+    for j in range(nt):
+        here = (s == t) & (t == j)
+        pl.when(jnp.logical_not(here))(lambda j=j: first_copy(j).start())
+        pl.when(here)(lambda j=j: first_here(j).start())
+
+    key = shifts_ref.shape[1]
+
+    def shift_copy(u, j):
+        return remote(
+            shift_ref.at[:, pl.ds(j * key, key)], shifts_ref.at[pl.ds(s * rows, rows)],
+            d_send.at[j], d_recv.at[s], {"sp": u},
+        )
+
+    def shift_here(j):
+        return pltpu.make_async_copy(
+            shift_ref.at[:, pl.ds(j * key, key)], shifts_ref.at[pl.ds(s * rows, rows)], d_local
+        )
+
+    recs = [(u, j) for u, (kind, j) in enumerate(roles) if kind == "rec"]
+    for u, j in recs:
+        pl.when(s != u)(lambda u=u, j=j: shift_copy(u, j).start())
+        pl.when(s == u)(lambda j=j: shift_here(j).start())
+
+    def second_copy(k, d):
+        return remote(
+            tbuf.at[k, t], tbuf.at[k, t], b_send.at[k, d], b_recv.at[k, d],
+            {"tp": lax.rem(t + d, nt)},
+        )
+
+    for k in range(n):
+        here = (s == k) & (t == k)
+
+        def arrived(k=k):
+            remote(
+                tok_ref.at[pl.ds(0, piece)], tbuf.at[k, t], a_send.at[0], a_recv.at[k],
+                {"sp": t, "tp": t},
+            ).wait_recv()
+
+        pl.when(jnp.logical_not(here))(arrived)
+        pl.when(here)(lambda k=k: first_here(k).wait())
+        for d in range(1, nt):
+            second_copy(k, d).start()
+
+    gain = gain_ref[:, pl.ds(pl.multiple_of(s * feats, feats), feats)]
+    for k in range(n):
+        for d in range(1, nt):
+            second_copy(k, d).wait_recv()
+        raw = tbuf[k].reshape(rows, feats).astype(jnp.float32)
+        scaled[pl.ds(k * rows, rows)] = (raw * gain).astype(jnp.bfloat16)
+        total = jnp.sum(raw * raw, axis=1, keepdims=True)
+        flat = jnp.transpose(jnp.broadcast_to(total, (rows, 128)))
+        squares[s, :, pl.ds(k * rows, rows)] = flat[:8]
+
+    def square_copy(a):
+        return remote(
+            squares.at[s], squares.at[s], q_send.at[a], q_recv.at[a], {"sp": lax.rem(s + a, n)}
+        )
+
+    for a in range(1, n):
+        square_copy(a).start()
+
+    half = seq // HALVES
+
+    def right_copy(u, h):
+        at = (u, pl.ds(h * half, half), pl.ds(0, width[u]))
+        return remote(
+            send_r.at[at], recv_r.at[at], rs_sem.at[u, h], rr_sem.at[u, h],
+            {"sp": jnp.minimum(s + 1, n - 1)},
+        )
+
+    def left_copy(u, h):
+        at = (u, pl.ds(h * half, half), pl.ds(0, width[u]))
+        return remote(
+            send_l.at[at], recv_l.at[at], ls_sem.at[u, h], lr_sem.at[u, h],
+            {"sp": jnp.maximum(s - 1, 0)},
+        )
+
+    order = []
+    for i in range(n // 2):
+        order += [n - 1 - i, i]
+    for u in order:
+        kind, j = roles[u]
+        if kind == "att":
+            group = aq_ref.shape[0] // ak_ref.shape[0]
+            pieces = [
+                aq_ref[pl.ds(j * group * HEAD, group * HEAD)],
+                ak_ref[pl.ds(j * HEAD, HEAD)],
+                av_ref[pl.ds(j * HEAD, HEAD)],
+            ]
+        else:
+            pieces = [
+                rq_ref[pl.ds(j * REC_KEY, REC_KEY)],
+                rf_ref[pl.ds(j * REC_KEY, REC_KEY)],
+                ri_ref[pl.ds(j * REC_VAL, REC_VAL)],
+            ]
+        weight = jnp.concatenate(pieces, axis=0)
+        for h in range(HALVES):
+            at = (u, pl.ds(h * half, half), pl.ds(0, width[u]))
+            product = dot_nt(scaled[pl.ds(h * half, half)], weight)
+            part[at] = product
+            if u > 0:
+                @pl.when(s == 0)
+                def _():
+                    send_r[at] = product.astype(jnp.bfloat16)
+                    right_copy(u, h).start()
+            if u < n - 1:
+                @pl.when(s == n - 1)
+                def _():
+                    send_l[at] = product.astype(jnp.bfloat16)
+                    left_copy(u, h).start()
+
+    for i in range(n - 1):
+        for h in range(HALVES):
+            u = n - 1 - i
+            at = (u, pl.ds(h * half, half), pl.ds(0, width[u]))
+
+            @pl.when((s > 0) & (s < u))
+            def _():
+                right_copy(u, h).wait_recv()
+                send_r[at] = (part[at] + recv_r[at].astype(jnp.float32)).astype(jnp.bfloat16)
+                right_copy(u, h).start()
+
+            v = i
+            bt = (v, pl.ds(h * half, half), pl.ds(0, width[v]))
+
+            @pl.when((s < n - 1) & (s > v))
+            def _():
+                left_copy(v, h).wait_recv()
+                send_l[bt] = (part[bt] + recv_l[bt].astype(jnp.float32)).astype(jnp.bfloat16)
+                left_copy(v, h).start()
+
+    for a in range(1, n):
+        square_copy(a).wait_recv()
+    total = squares[0, :1]
+    for k in range(1, n):
+        total = total + squares[k, :1]
+    inv_rms = lax.rsqrt(total / gain_ref.shape[1] + EPS)
+    inv_rms = jnp.transpose(jnp.broadcast_to(inv_rms, (128, seq)))
+    for u in range(n):
+        @pl.when(s == u)
+        def _():
+            for h in range(HALVES):
+                at = (u, pl.ds(h * half, half), pl.ds(0, width[u]))
+                result = part[at]
+                if u > 0:
+                    right_copy(u, h).wait_recv()
+                    result = result + recv_r[at].astype(jnp.float32)
+                if u < n - 1:
+                    left_copy(u, h).wait_recv()
+                    result = result + recv_l[at].astype(jnp.float32)
+                factor = inv_rms[h * half:(h + 1) * half]
+                for c in range(width[u] // 128):
+                    out_ref[pl.ds(h * half, half), pl.ds(c * 128, 128)] = (
+                        result[:, c * 128:(c + 1) * 128] * factor
+                    ).astype(jnp.bfloat16)
+
+    for j in range(nt):
+        here = (s == t) & (t == j)
+        pl.when(jnp.logical_not(here))(lambda j=j: first_copy(j).wait_send())
+    for u, j in recs:
+        pl.when(s != u)(lambda u=u, j=j: shift_copy(u, j).wait_send())
+
+        @pl.when(s == u)
+        def _():
+            shift_here(j).wait()
+            for k in range(n):
+                if k != u:
+                    remote(
+                        shift_ref.at[:, pl.ds(j * key, key)], shifts_ref.at[pl.ds(k * rows, rows)],
+                        d_send.at[j], d_recv.at[k], {"sp": k},
+                    ).wait_recv()
+    for k in range(n):
+        for d in range(1, nt):
+            second_copy(k, d).wait_send()
+    for a in range(1, n):
+        square_copy(a).wait_send()
+    for u in range(n):
+        for h in range(HALVES):
+            if u > 0:
+                pl.when(s < u)(lambda u=u, h=h: right_copy(u, h).wait_send())
+            if u < n - 1:
+                pl.when(s > u)(lambda u=u, h=h: left_copy(u, h).wait_send())
+
+
+def stick_mixer(j, group, x_ref, offset_ref, out_ref):
+    seq = x_ref.shape[0]
+    block = min(128, seq)
+    low = lax.broadcasted_iota(jnp.int32, (block, block), 0)
+    high = lax.broadcasted_iota(jnp.int32, (block, block), 1)
+    later = (low > high).astype(jnp.bfloat16)
+    visible = jnp.concatenate([high < low] * group, axis=0)
+    offset = jnp.concatenate(
+        [jnp.full((block, block), offset_ref[j * group + g], jnp.float32) for g in range(group)],
+        axis=0,
+    )
+    keys = x_ref[:, group * HEAD:(group + 1) * HEAD]
+    values = x_ref[:, (group + 1) * HEAD:(group + 2) * HEAD]
+    for q in range(seq // block):
+        queries = x_ref[q * block:(q + 1) * block, :group * HEAD]
+        queries = jnp.concatenate(
+            [queries[:, g * HEAD:(g + 1) * HEAD] for g in range(group)], axis=0
+        )
+        run = jnp.zeros((group * block, 1), jnp.float32)
+        summed = jnp.zeros((group * block, HEAD), jnp.float32)
+        for c in range(q, -1, -1):
+            at = slice(c * block, (c + 1) * block)
+            score = dot_nt(queries, keys[at]) * HEAD ** (-0.5) + offset
+            keep = -(jnp.maximum(score, 0.0) + jnp.log1p(jnp.exp(-jnp.abs(score))))
+            gate = score + keep
+            if c == q:
+                keep = jnp.where(visible, keep, 0.0)
+            top = keep.astype(jnp.bfloat16)
+            rest = (keep - top.astype(jnp.float32)).astype(jnp.bfloat16)
+            tail = dot_nn(top, later) + dot_nn(rest, later)
+            weight = jnp.exp(gate + tail + run)
+            if c == q:
+                weight = jnp.where(visible, weight, 0.0)
+            summed = summed + dot_nn(weight.astype(jnp.bfloat16), values[at])
+            run = run + jnp.sum(keep, axis=1, keepdims=True)
+        out_ref[q * block:(q + 1) * block] = jnp.concatenate(
+            [summed[g * block:(g + 1) * block] for g in range(group)], axis=1
+        ).astype(jnp.bfloat16)
+
+
+def state_mixer(j, x_ref, bound_ref, shift_ref, gain_ref, out_ref):
+    seq = x_ref.shape[0]
+    block = min(128, seq)
+    bound = bound_ref[:, pl.ds(pl.multiple_of(j * REC_KEY, REC_KEY), REC_KEY)]
+    gain = gain_ref[:, pl.ds(pl.multiple_of(j * REC_VAL, REC_VAL), REC_VAL)]
+    gap = 1.0 - bound
+    low = lax.broadcasted_iota(jnp.int32, (block, block), 0)
+    high = lax.broadcasted_iota(jnp.int32, (block, block), 1)
+    upto = ((high <= low) & (high // STEP == low // STEP)).astype(jnp.float32)
+    lower = (
+        lax.broadcasted_iota(jnp.int32, (STEP, STEP), 0)
+        >= lax.broadcasted_iota(jnp.int32, (STEP, STEP), 1)
+    )
+    state = jnp.zeros((REC_VAL, REC_KEY), jnp.float32)
+    for b in range(seq // block):
+        at = slice(b * block, (b + 1) * block)
+        logit = x_ref[at, REC_KEY:2 * REC_KEY].astype(jnp.float32)
+        query = x_ref[at, :REC_KEY].astype(jnp.float32)
+        value = x_ref[at, 2 * REC_KEY:2 * REC_KEY + REC_VAL]
+        log_decay = jnp.log(bound + gap * jax.nn.sigmoid(logit)) + shift_ref[at]
+        keyed = gap * jax.nn.sigmoid(-logit)
+        query = query * jax.nn.sigmoid(query)
+        running = jnp.dot(
+            upto, log_decay, precision=TOP_PRECISION, preferred_element_type=jnp.float32
+        )
+        for i in range(block // STEP):
+            it = slice(i * STEP, (i + 1) * STEP)
+            cumulative, q, k, v = running[it], query[it], keyed[it], value[it]
+            middle = cumulative[STEP // 2 - 1:STEP // 2]
+            last = cumulative[STEP - 1:STEP]
+            score = dot_nt(
+                (q * jnp.exp(cumulative - middle)).astype(jnp.bfloat16),
+                (k * jnp.exp(middle - cumulative)).astype(jnp.bfloat16),
+            )
+            score = jnp.where(lower, score, 0.0).astype(jnp.bfloat16)
+            raw = dot_nn(score, v) + dot_nt(
+                (q * jnp.exp(cumulative)).astype(jnp.bfloat16), state.astype(jnp.bfloat16)
+            )
+            state = state * jnp.exp(last) + dot_tn(
+                v, (k * jnp.exp(last - cumulative)).astype(jnp.bfloat16)
+            )
+            scale = lax.rsqrt(jnp.mean(raw * raw, axis=1, keepdims=True) + EPS)
+            out_ref[b * block + i * STEP:b * block + (i + 1) * STEP] = (
+                raw * scale * gain
+            ).astype(jnp.bfloat16)
+
+
+def mix_kernel(roles, group, x_ref, offset_ref, bound_ref, shift_ref, gain_ref, out_ref):
+    s = lax.axis_index("sp")
+    j = select_static(s, [index for _, index in roles])
+    is_rec = select_static(s, [int(kind == "rec") for kind, _ in roles])
+
+    @pl.when(is_rec == 0)
+    def _():
+        stick_mixer(j, group, x_ref, offset_ref, out_ref)
+
+    @pl.when(is_rec == 1)
+    def _():
+        state_mixer(j, x_ref, bound_ref, shift_ref, gain_ref, out_ref)
+
+
+def output_kernel(
+    roles, n, nt,
+    x_ref, wa_ref, wr_ref, out_ref,
+    heads, part, landed, mixed,
+    e_send, e_recv, e_local, f_send, f_recv, g_send, g_recv, g_local,
+):
+    s, t = lax.axis_index("sp"), lax.axis_index("tp")
+    seq, wide = x_ref.shape
+    piece = seq // (n * nt)
+    cols = wa_ref.shape[1]
+
+    barrier = pltpu.get_barrier_semaphore()
+    for a in range(1, n):
+        pl.semaphore_signal(
+            barrier, inc=1, device_id={"sp": lax.rem(s + a, n)}, device_id_type=MESH
+        )
+    for b in range(1, nt):
+        pl.semaphore_signal(
+            barrier, inc=1, device_id={"tp": lax.rem(t + b, nt)}, device_id_type=MESH
+        )
+    pl.semaphore_wait(barrier, n + nt - 2)
+
+    def head_copy(a):
+        return remote(
+            x_ref, heads.at[s], e_send.at[a], e_recv.at[a], {"sp": lax.rem(s + a, n)}
+        )
+
+    own = pltpu.make_async_copy(x_ref, heads.at[s], e_local)
+    own.start()
+    for a in range(1, n):
+        head_copy(a).start()
+    own.wait()
+    for a in range(1, n):
+        head_copy(a).wait_recv()
+
+    total = None
+    for u, (kind, j) in enumerate(roles):
+        ref = wa_ref if kind == "att" else wr_ref
+        term = dot_nn(heads[u], ref[pl.ds(j * wide, wide)])
+        total = term if total is None else total + term
+    part[...] = total.astype(jnp.bfloat16).reshape(n, nt, piece, cols)
+
+    def share_copy(b):
+        to = lax.rem(t + b, nt)
+        return remote(
+            part.at[:, to], landed.at[b], f_send.at[b], f_recv.at[b], {"tp": to}
+        )
+
+    for b in range(1, nt):
+        share_copy(b).start()
+    result = part[:, t].astype(jnp.float32)
+    for b in range(1, nt):
+        share_copy(b).wait_recv()
+        result = result + landed[b].astype(jnp.float32)
+    mixed[...] = result.astype(jnp.bfloat16)
+
+    place = out_ref.at[:, pl.ds(pl.multiple_of(s * cols, cols), cols)]
+
+    def final_copy(a):
+        to = lax.rem(s + a, n)
+        return remote(mixed.at[to], place, g_send.at[a], g_recv.at[a], {"sp": to})
+
+    here = pltpu.make_async_copy(mixed.at[s], place, g_local)
+    for a in range(1, n):
+        final_copy(a).start()
+    here.start()
+    here.wait()
+    for a in range(1, n):
+        remote(
+            mixed.at[s],
+            out_ref.at[:, pl.ds(pl.multiple_of(lax.rem(s + n - a, n) * cols, cols), cols)],
+            g_send.at[a], g_recv.at[a], {"sp": lax.rem(s + a, n)},
+        ).wait_recv()
+    for a in range(1, n):
+        head_copy(a).wait_send()
+        final_copy(a).wait_send()
+    for b in range(1, nt):
+        share_copy(b).wait_send()
+
+
+def stationary_fits(args):
+    n, nt = lax.axis_size("sp"), lax.axis_size("tp")
+    tokens, att_q, att_k, rec_q, rec_i = args[0], args[2], args[3], args[5], args[7]
+    rows, feats = tokens.shape
+    att_count, rec_count = att_k.shape[0] // HEAD, rec_i.shape[0] // REC_VAL
+    group = att_q.shape[0] // att_k.shape[0]
+    return (
+        n == nt
+        and n % 2 == 0
+        and att_count + rec_count == n
+        and group * HEAD == REC_VAL
+        and feats == att_q.shape[1]
+        and rows % 128 == 0
+        and rows * n <= 1024
+    )
+
+
+def stationary(
+    tokens, norm_gain, att_q_weight, att_k_weight, att_v_weight, rec_q_weight, rec_f_weight,
+    rec_i_weight, att_out_weight, rec_out_weight, score_offset, lower_bound, decay_shift, rec_gain,
+):
+    n, nt = lax.axis_size("sp"), lax.axis_size("tp")
+    rows, feats = tokens.shape
+    seq = rows * n
+    cols = att_out_weight.shape[1]
+    group = att_q_weight.shape[0] // att_k_weight.shape[0]
+    roles = role_table(n, att_k_weight.shape[0] // HEAD, rec_i_weight.shape[0] // REC_VAL)
+    width = [(group + 2) * HEAD if kind == "att" else 2 * REC_KEY + REC_VAL for kind, _ in roles]
+    widest = max(width)
+    bf16, f32 = jnp.bfloat16, jnp.float32
+    dma = pltpu.SemaphoreType.DMA
+    vmem = pl.BlockSpec(memory_space=pltpu.VMEM)
+    smem = pl.BlockSpec(memory_space=pltpu.SMEM)
+    projected, shifts = pl.pallas_call(
+        functools.partial(project_kernel, roles, n, nt, width),
+        out_shape=(
+            jax.ShapeDtypeStruct((seq, widest), bf16),
+            jax.ShapeDtypeStruct((seq, REC_KEY), f32),
+        ),
+        in_specs=[vmem] * 9,
+        out_specs=(vmem, vmem),
+        scratch_shapes=[
+            pltpu.VMEM((n, nt, rows // nt, feats), bf16),
+            pltpu.VMEM((n, 8, seq), f32),
+            pltpu.VMEM((seq, feats), bf16),
+            pltpu.VMEM((n, seq, widest), f32),
+            pltpu.VMEM((n, seq, widest), bf16),
+            pltpu.VMEM((n, seq, widest), bf16),
+            pltpu.VMEM((n, seq, widest), bf16),
+            pltpu.VMEM((n, seq, widest), bf16),
+            dma((nt,)), dma((n,)), dma, dma((n, nt)), dma((n, nt)),
+            dma((n,)), dma((n,)), dma, dma((n,)), dma((n,)),
+            dma((n, HALVES)), dma((n, HALVES)), dma((n, HALVES)), dma((n, HALVES)),
+        ],
+        compiler_params=pltpu.CompilerParams(collective_id=0, has_side_effects=True),
+        name="project",
+    )(
+        tokens, norm_gain.reshape(1, -1), att_q_weight, att_k_weight, att_v_weight,
+        rec_q_weight, rec_f_weight, rec_i_weight, decay_shift,
+    )
+    heads = pl.pallas_call(
+        functools.partial(mix_kernel, roles, group),
+        out_shape=jax.ShapeDtypeStruct((seq, REC_VAL), bf16),
+        in_specs=[vmem, smem, vmem, vmem, vmem],
+        out_specs=vmem,
+        name="mix",
+    )(projected, score_offset, lower_bound.reshape(1, -1), shifts, rec_gain.reshape(1, -1))
+    return pl.pallas_call(
+        functools.partial(output_kernel, roles, n, nt),
+        out_shape=jax.ShapeDtypeStruct((seq // (n * nt), cols * n), bf16),
+        in_specs=[vmem] * 3,
+        out_specs=vmem,
+        scratch_shapes=[
+            pltpu.VMEM((n, seq, REC_VAL), bf16),
+            pltpu.VMEM((n, nt, seq // (n * nt), cols), bf16),
+            pltpu.VMEM((nt, n, seq // (n * nt), cols), bf16),
+            pltpu.VMEM((n, seq // (n * nt), cols), bf16),
+            dma((n,)), dma((n,)), dma, dma((nt,)), dma((nt,)), dma((n,)), dma((n,)), dma,
+        ],
+        compiler_params=pltpu.CompilerParams(collective_id=1, has_side_effects=True),
+        name="output",
+    )(heads, att_out_weight, rec_out_weight)
+
+
+def on_device(*args):
+    if stationary_fits(args):
+        return stationary(*args)
+    return gathered_plan(*args)
+
+
 def solution(mesh):
     in_specs = (
         P(("grp", "sp"), "tp"),

time: 230 us -> 89 us (0.39)
  blocking collectives: 92.5 us -> 0 us
  Pallas kernels: 0 us -> 86.8 us
  waiting for transfers between devices: 69.5 us -> 0 us
  matrix products: 29.5 us -> 0 us
  other arithmetic: 21.6 us -> 0 us
  between operations: 13.8 us -> 0.02 us
    all_gather x6 -> x0, blocking collectives: 92.5 us -> none  [the longest x2 25.2 us: entering(): lax.all_gather(part.astype(kind), axis)]
    pallas_call x0 -> x3, Pallas kernels: none -> 86.8 us  [the longest x1 56.8 us: stationary(): pl.pallas_call(functools.partial(project_kernel, roles, n, nt, width), ou...]
    all_gather x6 -> x0, waiting for transfers between devices: 44.6 us -> none  [the longest x1 27.1 us: on_device(): lax.all_gather(rec_i_weight, 'sp', axis=1, tiled=True)]
    dot_general x18 -> x0, matrix products: 28.4 us -> none  [the longest x2 13.3 us: block_pass(): jnp.einsum('thk,tshk,shk->ths', query_rows, decay, keyed_values, precisio...]
    reduce_scatter x1 -> x0, waiting for transfers between devices: 21.2 us -> none  [on_device(): lax.psum_scatter((jnp.dot(att_out, att_rows, preferred_element_type=jnp.f...]
    dot_general x2 -> x0, other arithmetic: 11.8 us -> none  [block_pass(): jnp.einsum('thk,tshk,shk->ths', query_rows, decay, keyed_values, precisio...]
    another operation x7 -> x0, other arithmetic: 6.13 us -> none
    unnamed x7 -> x0, waiting for transfers between devices: 3.68 us -> none
  transfers between devices with their start and end apart: 7 -> 0, of which waited for: 3 -> 0; matrix products, arithmetic and copies ran while one was open for 22% -> 0% of each run, Pallas kernels for 0% -> 0%
where the time goes in v1:
time: 89 us; the launch traced here: 88.4 us
  Pallas kernels  86.8 us (98%)
  local copies, waits for them, and re-layouts  1.57 us (2%)
    pallas_call x1, Pallas kernels, stationary(): pl.pallas_call(functools.partial(project_kernel, roles, n, nt, width), ou...  56.8 us
    pallas_call x1, Pallas kernels, stationary(): pl.pallas_call(functools.partial(output_kernel, roles, n, nt), out_shape=...  25.4 us
    pallas_call x1, Pallas kernels, stationary(): pl.pallas_call(functools.partial(mix_kernel, roles, group), out_shape=jax...  4.59 us

profile of v1, /device:TPU:0, one launch (start us, length us, event | category | flops | bytes accessed | tf_op | source)
XLA Modules:
  0.0 88.4 jit_solution(7099604529178295967)
XLA Ops:
  0.0 56.8 %project.1 = (bf16[512,384]{1,0:T(8,128)(2,1)}, f32[512,128]{1,0:T(8,128)}) custom-call(bf16[128,512]{1,0:T(8,128)(2,1)} %tok_ref.1, f32[1,2048]{1,0:T(1,128)} %bitcast.3, bf16[256,512]{1,0:T(8,128)(2,1)} %aq_ref.1, bf16[128,512]{1,0:T(8,128)(2,1)} %ak_ref.1, bf16[128,512]{1,0:T(8,128)(2,1)} %av_ref.1, bf16[256,512]{1,0:T(8,128)(2,1)} %rq_ref.1, ...), custom_call_target="tpu_custom_call" | custom-call | tf_op jit(solution)/shard_map/project/pallas_call | solution.py:713
  56.8 4.6 %mix.1.x_ref = bf16[512,128]{1,0:T(8,128)(2,1)} custom-call(bf16[512,384]{1,0:T(8,128)(2,1)} %get-tuple-element.7.x_ref, f32[4]{0:T(128)} %offset_ref.1, f32[1,256]{1,0:T(1,128)} %bitcast.4, f32[512,128]{1,0:T(8,128)} %get-tuple-element.8.shift_ref, f32[1,256]{1,0:T(1,128)} %bitcast.5), custom_call_target="tpu_custom_call" | custom-call | tf_op jit(solution)/shard_map/mix/pallas_call | solution.py:740
  61.4 25.4 %output.1 = bf16[32,2048]{1,0:T(8,128)(2,1)} custom-call(bf16[512,128]{1,0:T(8,128)(2,1)} %mix.1.x_ref, bf16[256,512]{1,0:T(8,128)(2,1)} %wa_ref.1, bf16[256,512]{1,0:T(8,128)(2,1)} %wr_ref.1), custom_call_target="tpu_custom_call" | custom-call | tf_op jit(solution)/shard_map/output/pallas_call | solution.py:747
  86.8 1.6 %copy.16 = bf16[32,2048]{1,0:T(8,128)(2,1)} copy(bf16[32,2048]{1,0:T(8,128)(2,1)} %output.1) | data formatting | bytes 262144

commit v2 on v0

--- a/solution.py
+++ b/solution.py
@@ -1,6 +1,10 @@
+import functools
+
 import jax
 import jax.numpy as jnp
 from jax import lax
+from jax.experimental import pallas as pl
+from jax.experimental.pallas import tpu as pltpu
 from jax.sharding import PartitionSpec as P
 
 HEAD = 64
@@ -181,7 +185,7 @@
     return rescaled_input.reshape(rows, heads * REC_VAL).astype(jnp.bfloat16)
 
 
-def on_device(
+def gathered_plan(
     tokens,
     norm_gain,
     att_q_weight,
@@ -229,6 +233,467 @@
     )
 
 
+MESH = pl.DeviceIdType.MESH
+STEP = 32
+
+
+def dot_nt(a, b):
+    return lax.dot_general(a, b, (((1,), (1,)), ((), ())), preferred_element_type=jnp.float32)
+
+
+def dot_tn(a, b):
+    return lax.dot_general(a, b, (((0,), (0,)), ((), ())), preferred_element_type=jnp.float32)
+
+
+def dot_nn(a, b):
+    return jnp.dot(a, b, preferred_element_type=jnp.float32)
+
+
+def remote(src, dst, send_sem, recv_sem, target):
+    return pltpu.make_async_remote_copy(
+        src_ref=src,
+        dst_ref=dst,
+        send_sem=send_sem,
+        recv_sem=recv_sem,
+        device_id=target,
+        device_id_type=MESH,
+    )
+
+
+SUB = 64
+
+
+def stick_block(q, j, group, x, offset_ref):
+    block = 128
+    low = lax.broadcasted_iota(jnp.int32, (block, block), 0)
+    high = lax.broadcasted_iota(jnp.int32, (block, block), 1)
+    later = (low > high).astype(jnp.bfloat16)
+    visible = jnp.concatenate([high < low] * group, axis=0)
+    offset = jnp.concatenate(
+        [jnp.full((block, block), offset_ref[j * group + g], jnp.float32) for g in range(group)],
+        axis=0,
+    )
+    queries = x[q * block:(q + 1) * block, :group * HEAD]
+    queries = jnp.concatenate([queries[:, g * HEAD:(g + 1) * HEAD] for g in range(group)], axis=0)
+    run = jnp.zeros((group * block, 1), jnp.float32)
+    summed = jnp.zeros((group * block, HEAD), jnp.float32)
+    for c in range(q, -1, -1):
+        keys = x[c * block:(c + 1) * block, group * HEAD:(group + 1) * HEAD]
+        values = x[c * block:(c + 1) * block, (group + 1) * HEAD:(group + 2) * HEAD]
+        score = dot_nt(queries, keys) * HEAD ** (-0.5) + offset
+        keep = -(jnp.maximum(score, 0.0) + jnp.log1p(jnp.exp(-jnp.abs(score))))
+        gate = score + keep
+        if c == q:
+            keep = jnp.where(visible, keep, 0.0)
+        top = keep.astype(jnp.bfloat16)
+        rest = (keep - top.astype(jnp.float32)).astype(jnp.bfloat16)
+        tail = dot_nn(top, later) + dot_nn(rest, later)
+        weight = jnp.exp(gate + tail + run)
+        if c == q:
+            weight = jnp.where(visible, weight, 0.0)
+        summed = summed + dot_nn(weight.astype(jnp.bfloat16), values)
+        run = run + jnp.sum(keep, axis=1, keepdims=True)
+    return jnp.concatenate(
+        [summed[g * block:(g + 1) * block] for g in range(group)], axis=1
+    ).astype(jnp.bfloat16)
+
+
+def state_block(b, j, x, first, bound_ref, shift_ref, gain_ref, state_ref):
+    block = 128
+    bound = bound_ref[:, pl.ds(pl.multiple_of(j * REC_KEY, REC_KEY), REC_KEY)]
+    gain = gain_ref[:, pl.ds(pl.multiple_of(j * REC_VAL, REC_VAL), REC_VAL)]
+    gap = 1.0 - bound
+    low = lax.broadcasted_iota(jnp.int32, (block, block), 0)
+    high = lax.broadcasted_iota(jnp.int32, (block, block), 1)
+    upto = ((high <= low) & (high // STEP == low // STEP)).astype(jnp.float32)
+    lower = (
+        lax.broadcasted_iota(jnp.int32, (STEP, STEP), 0)
+        >= lax.broadcasted_iota(jnp.int32, (STEP, STEP), 1)
+    )
+    state = jnp.zeros((REC_VAL, REC_KEY), jnp.float32) if b == 0 else state_ref[...]
+    at = slice(b * block, (b + 1) * block)
+    query = x[at, first:first + REC_KEY].astype(jnp.float32)
+    logit = x[at, first + REC_KEY:first + 2 * REC_KEY].astype(jnp.float32)
+    value = x[at, first + 2 * REC_KEY:first + 2 * REC_KEY + REC_VAL]
+    log_decay = jnp.log(bound + gap * jax.nn.sigmoid(logit)) + shift_ref[at]
+    keyed = gap * jax.nn.sigmoid(-logit)
+    query = query * jax.nn.sigmoid(query)
+    running = jnp.dot(upto, log_decay, precision=TOP_PRECISION, preferred_element_type=jnp.float32)
+    outs = []
+    for i in range(block // STEP):
+        it = slice(i * STEP, (i + 1) * STEP)
+        cumulative, q, k, v = running[it], query[it], keyed[it], value[it]
+        middle = cumulative[STEP // 2 - 1:STEP // 2]
+        last = cumulative[STEP - 1:STEP]
+        score = dot_nt(
+            (q * jnp.exp(cumulative - middle)).astype(jnp.bfloat16),
+            (k * jnp.exp(middle - cumulative)).astype(jnp.bfloat16),
+        )
+        score = jnp.where(lower, score, 0.0).astype(jnp.bfloat16)
+        raw = dot_nn(score, v) + dot_nt(
+            (q * jnp.exp(cumulative)).astype(jnp.bfloat16), state.astype(jnp.bfloat16)
+        )
+        state = state * jnp.exp(last) + dot_tn(
+            v, (k * jnp.exp(last - cumulative)).astype(jnp.bfloat16)
+        )
+        scale = lax.rsqrt(jnp.mean(raw * raw, axis=1, keepdims=True) + EPS)
+        outs.append((raw * scale * gain).astype(jnp.bfloat16))
+    state_ref[...] = state
+    return jnp.concatenate(outs, axis=0)
+
+
+def layer_kernel(
+    n, nt, group,
+    tok_ref, gain_ref, aq_ref, ak_ref, av_ref, rq_ref, rf_ref, ri_ref, shift_ref,
+    wa_ref, wr_ref, offset_ref, bound_ref, rec_gain_ref,
+    out_ref,
+    tbuf, shifts, squares, part, sent, came, x, state, heads, shares, landed, mixed,
+    a_send, a_recv, a_local, b_send, b_recv, d_send, d_recv, d_local, q_send, q_recv,
+    c_send, c_recv, e_send, e_recv, f_send, f_recv, g_send, g_recv, g_local,
+):
+    s, t = lax.axis_index("sp"), lax.axis_index("tp")
+    rows, feats = tok_ref.shape
+    piece = rows // nt
+    width = x.shape[1]
+    att_width = (group + 2) * HEAD
+    wide = group * HEAD
+    cols = wa_ref.shape[1]
+    subs = rows // SUB
+    ends = (0, n - 1)
+    at_end = (s == 0) | (s == n - 1)
+    e = s // (n - 1)
+    f32, bf16 = jnp.float32, jnp.bfloat16
+
+    barrier = pltpu.get_barrier_semaphore()
+    for a in range(n):
+        for b in range(nt):
+            if a or b:
+                pl.semaphore_signal(
+                    barrier, inc=1,
+                    device_id={"sp": lax.rem(s + a, n), "tp": lax.rem(t + b, nt)},
+                    device_id_type=MESH,
+                )
+    pl.semaphore_wait(barrier, n * nt - 1)
+
+    def first_copy(j):
+        return remote(
+            tok_ref.at[pl.ds(j * piece, piece)], tbuf.at[s, j], a_send.at[j], a_recv.at[s],
+            {"sp": t, "tp": j},
+        )
+
+    def first_here(j):
+        return pltpu.make_async_copy(
+            tok_ref.at[pl.ds(j * piece, piece)], tbuf.at[s, j], a_local
+        )
+
+    for j in range(nt):
+        here = (s == t) & (t == j)
+        pl.when(jnp.logical_not(here))(lambda j=j: first_copy(j).start())
+        pl.when(here)(lambda j=j: first_here(j).start())
+
+    def shift_copy(i):
+        return remote(
+            shift_ref.at[:, pl.ds(i * REC_KEY, REC_KEY)], shifts.at[pl.ds(s * rows, rows)],
+            d_send.at[i], d_recv.at[s], {"sp": ends[i]},
+        )
+
+    def shift_here(i):
+        return pltpu.make_async_copy(
+            shift_ref.at[:, pl.ds(i * REC_KEY, REC_KEY)], shifts.at[pl.ds(s * rows, rows)], d_local
+        )
+
+    for i, u in enumerate(ends):
+        pl.when(s != u)(lambda i=i: shift_copy(i).start())
+        pl.when(s == u)(lambda i=i: shift_here(i).start())
+
+    def second_copy(k, d):
+        return remote(
+            tbuf.at[k, t], tbuf.at[k, t], b_send.at[k, d], b_recv.at[k, d],
+            {"tp": lax.rem(t + d, nt)},
+        )
+
+    def relay(k):
+        here = (s == k) & (t == k)
+
+        def arrived():
+            remote(
+                tok_ref.at[pl.ds(0, piece)], tbuf.at[k, t], a_send.at[0], a_recv.at[k],
+                {"sp": t, "tp": t},
+            ).wait_recv()
+
+        pl.when(jnp.logical_not(here))(arrived)
+        pl.when(here)(lambda: first_here(k).wait())
+        for d in range(1, nt):
+            second_copy(k, d).start()
+
+    gain = gain_ref[:, pl.ds(pl.multiple_of(s * feats, feats), feats)]
+
+    def square_copy(k, i):
+        return remote(
+            squares.at[s, k], squares.at[s, k], q_send.at[k, i], q_recv.at[s, k], {"sp": ends[i]}
+        )
+
+    def chain_copy(i, c):
+        to = jnp.maximum(s - 1, 0) if i == 0 else jnp.minimum(s + 1, n - 1)
+        return remote(
+            sent.at[i, pl.ds(c * SUB, SUB)], came.at[i, pl.ds(c * SUB, SUB)],
+            c_send.at[i, c], c_recv.at[i, c], {"sp": to},
+        )
+
+    weights = []
+    for i in range(2):
+        weights.append(jnp.concatenate(
+            [
+                aq_ref[pl.ds(i * wide, wide)],
+                ak_ref[pl.ds(i * HEAD, HEAD)],
+                av_ref[pl.ds(i * HEAD, HEAD)],
+                rq_ref[pl.ds(i * REC_KEY, REC_KEY)],
+                rf_ref[pl.ds(i * REC_KEY, REC_KEY)],
+                ri_ref[pl.ds(i * REC_VAL, REC_VAL)],
+            ],
+            axis=0,
+        ))
+
+    def project(k):
+        for d in range(1, nt):
+            second_copy(k, d).wait_recv()
+        raw = tbuf[k].reshape(rows, feats).astype(f32)
+        scaled = (raw * gain).astype(bf16)
+        for i in range(2):
+            product = dot_nt(scaled, weights[i])
+            part[i, pl.ds(k * rows, rows)] = product
+
+            @pl.when(s == ends[1 - i])
+            def _():
+                for r in range(subs):
+                    c = k * subs + r
+                    sent[i, pl.ds(c * SUB, SUB)] = product[r * SUB:(r + 1) * SUB].astype(bf16)
+                    chain_copy(i, c).start()
+
+        total = jnp.sum(raw * raw, axis=1, keepdims=True)
+        flat = jnp.transpose(jnp.broadcast_to(total, (rows, 128)))
+        squares[s, k] = flat[:8]
+        for i in range(2):
+            pl.when(s != ends[i])(lambda i=i: square_copy(k, i).start())
+
+    def forward(k):
+        for r in range(subs):
+            c = k * subs + r
+            for i in (1, 0):
+                chain_copy(i, c).wait_recv()
+                at = (i, pl.ds(c * SUB, SUB))
+                sent[at] = (part[at] + came[at].astype(f32)).astype(bf16)
+                chain_copy(i, c).start()
+
+    def head_copy(i, k, to):
+        at = (i, pl.ds(k * rows, rows))
+        return remote(
+            heads.at[at], heads.at[at], e_send.at[k, to], e_recv.at[i, k], {"sp": to}
+        )
+
+    def mix(k):
+        span = pl.ds(k * rows, rows)
+        for i in range(2):
+            @pl.when(s == ends[i])
+            def _():
+                for r in range(subs):
+                    chain_copy(i, k * subs + r).wait_recv()
+                for v in range(n):
+                    if v != ends[i]:
+                        remote(
+                            squares.at[v, k], squares.at[v, k], q_send.at[k, i], q_recv.at[v, k],
+                            {"sp": v},
+                        ).wait_recv()
+                if k == ends[i]:
+                    shift_here(i).wait()
+                else:
+                    remote(
+                        shift_ref.at[:, pl.ds(i * REC_KEY, REC_KEY)], shifts.at[span],
+                        d_send.at[i], d_recv.at[k], {"sp": k},
+                    ).wait_recv()
+        total = squares[0, k, :1]
+        for v in range(1, n):
+            total = total + squares[v, k, :1]
+        inv_rms = lax.rsqrt(total / gain_ref.shape[1] + EPS)
+        inv_rms = jnp.transpose(jnp.broadcast_to(inv_rms, (128, rows)))
+        for c in range(width // 128):
+            lane = pl.ds(c * 128, 128)
+            result = part[e, span, lane] + came[e, span, lane].astype(f32)
+            x[span, lane] = (result * inv_rms).astype(bf16)
+        heads[e, span, pl.ds(0, wide)] = stick_block(k, e, group, x, offset_ref)
+        heads[e, span, pl.ds(wide, REC_VAL)] = state_block(
+            k, e, x, att_width, bound_ref, shifts, rec_gain_ref, state
+        )
+        for i in range(2):
+            @pl.when(s == ends[i])
+            def _():
+                for to in (range(n - 1, 0, -1) if i == 0 else range(n - 1)):
+                    head_copy(i, k, to).start()
+
+    def share_copy(k, b):
+        to = lax.rem(t + b, nt)
+        return remote(
+            shares.at[k, to], landed.at[k, b], f_send.at[k, b], f_recv.at[k, b], {"tp": to}
+        )
+
+    def multiply(k):
+        span = pl.ds(k * rows, rows)
+        total = None
+        for i in range(2):
+            pl.when(s != ends[i])(lambda i=i: head_copy(i, k, ends[i]).wait_recv())
+        for i in range(2):
+            for ref, first, size in ((wa_ref, 0, wide), (wr_ref, wide, REC_VAL)):
+                term = dot_nn(heads[i, span, pl.ds(first, size)], ref[pl.ds(i * size, size)])
+                total = term if total is None else total + term
+        shares[k] = total.astype(bf16).reshape(nt, piece, cols)
+        for b in range(1, nt):
+            share_copy(k, b).start()
+
+    place = out_ref.at[:, pl.ds(pl.multiple_of(s * cols, cols), cols)]
+
+    def final_copy(k):
+        return remote(mixed.at[k], place, g_send.at[k], g_recv.at[s], {"sp": k})
+
+    def final_here(k):
+        return pltpu.make_async_copy(mixed.at[k], place, g_local)
+
+    def combine(k):
+        result = shares[k, t].astype(f32)
+        for b in range(1, nt):
+            share_copy(k, b).wait_recv()
+            result = result + landed[k, b].astype(f32)
+        mixed[k] = result.astype(bf16)
+        pl.when(s != k)(lambda: final_copy(k).start())
+        pl.when(s == k)(lambda: final_here(k).start())
+
+    relay(0)
+    for k in range(n):
+        if k + 1 < n:
+            relay(k + 1)
+        project(k)
+
+    @pl.when(jnp.logical_not(at_end))
+    def _():
+        for k in range(n):
+            forward(k)
+
+    @pl.when(at_end)
+    def _():
+        for k in range(n - 1):
+            mix(k)
+
+    multiply(0)
+
+    @pl.when(at_end)
+    def _():
+        mix(n - 1)
+
+    for k in range(1, n):
+        multiply(k)
+        combine(k - 1)
+    combine(n - 1)
+
+    for v in range(n):
+        @pl.when(s != v)
+        def _():
+            remote(
+                mixed.at[0], out_ref.at[:, pl.ds(v * cols, cols)], g_send.at[0], g_recv.at[v],
+                {"sp": v},
+            ).wait_recv()
+        pl.when(s == v)(lambda v=v: final_here(v).wait())
+
+    for j in range(nt):
+        here = (s == t) & (t == j)
+        pl.when(jnp.logical_not(here))(lambda j=j: first_copy(j).wait_send())
+    for i in range(2):
+        pl.when(s != ends[i])(lambda i=i: shift_copy(i).wait_send())
+    for k in range(n):
+        for d in range(1, nt):
+            second_copy(k, d).wait_send()
+            share_copy(k, d).wait_send()
+        for i in range(2):
+            pl.when(s != ends[i])(lambda i=i, k=k: square_copy(k, i).wait_send())
+
+            @pl.when(s == ends[i])
+            def _():
+                for to in range(n):
+                    if to != ends[i]:
+                        head_copy(i, k, to).wait_send()
+
+            @pl.when(s != ends[i])
+            def _():
+                for r in range(subs):
+                    chain_copy(i, k * subs + r).wait_send()
+        pl.when(s != k)(lambda k=k: final_copy(k).wait_send())
+
+
+def stationary_fits(args):
+    n, nt = lax.axis_size("sp"), lax.axis_size("tp")
+    tokens, att_q, att_k, rec_i = args[0], args[2], args[3], args[7]
+    rows, feats = tokens.shape
+    return (
+        n == nt
+        and n >= 3
+        and att_k.shape[0] // HEAD == 2
+        and rec_i.shape[0] // REC_VAL == 2
+        and (att_q.shape[0] // att_k.shape[0]) * HEAD == 128
+        and feats == att_q.shape[1]
+        and rows == 128
+    )
+
+
+def stationary(*args):
+    n, nt = lax.axis_size("sp"), lax.axis_size("tp")
+    tokens, norm_gain, att_q, att_k = args[:4]
+    score_offset, lower_bound, decay_shift, rec_gain = args[10:]
+    rows, feats = tokens.shape
+    seq = rows * n
+    cols = args[8].shape[1]
+    group = att_q.shape[0] // att_k.shape[0]
+    width = (group + 2) * HEAD + 2 * REC_KEY + REC_VAL
+    wide = group * HEAD + REC_VAL
+    piece = rows // nt
+    chunks = seq // SUB
+    bf16, f32 = jnp.bfloat16, jnp.float32
+    dma = pltpu.SemaphoreType.DMA
+    vmem = pl.BlockSpec(memory_space=pltpu.VMEM)
+    smem = pl.BlockSpec(memory_space=pltpu.SMEM)
+    return pl.pallas_call(
+        functools.partial(layer_kernel, n, nt, group),
+        out_shape=jax.ShapeDtypeStruct((piece, cols * n), bf16),
+        in_specs=[vmem] * 11 + [smem, vmem, vmem],
+        out_specs=vmem,
+        scratch_shapes=[
+            pltpu.VMEM((n, nt, piece, feats), bf16),
+            pltpu.VMEM((seq, REC_KEY), f32),
+            pltpu.VMEM((n, n, 8, rows), f32),
+            pltpu.VMEM((2, seq, width), f32),
+            pltpu.VMEM((2, seq, width), bf16),
+            pltpu.VMEM((2, seq, width), bf16),
+            pltpu.VMEM((seq, width), bf16),
+            pltpu.VMEM((REC_VAL, REC_KEY), f32),
+            pltpu.VMEM((2, seq, wide), bf16),
+            pltpu.VMEM((n, nt, piece, cols), bf16),
+            pltpu.VMEM((n, nt, piece, cols), bf16),
+            pltpu.VMEM((n, piece, cols), bf16),
+            dma((nt,)), dma((n,)), dma, dma((n, nt)), dma((n, nt)), dma((2,)), dma((n,)), dma,
+            dma((n, 2)), dma((n, n)), dma((2, chunks)), dma((2, chunks)),
+            dma((n, n)), dma((2, n)), dma((n, nt)), dma((n, nt)), dma((n,)), dma((n,)), dma,
+        ],
+        compiler_params=pltpu.CompilerParams(collective_id=0, has_side_effects=True),
+        name="layer",
+    )(
+        tokens, norm_gain.reshape(1, -1), *args[2:8], decay_shift, args[8], args[9],
+        score_offset, lower_bound.reshape(1, -1), rec_gain.reshape(1, -1),
+    )
+
+
+def on_device(*args):
+    if stationary_fits(args):
+        return stationary(*args)
+    return gathered_plan(*args)
+
+
 def solution(mesh):
     in_specs = (
         P(("grp", "sp"), "tp"),

time: 230 us -> 101 us (0.44)
  Pallas kernels: 0 us -> 98.3 us
  blocking collectives: 92.5 us -> 0 us
  waiting for transfers between devices: 69.5 us -> 0 us
  matrix products: 29.5 us -> 0 us
  other arithmetic: 21.6 us -> 0 us
  between operations: 13.8 us -> 0.01 us
    pallas_call x0 -> x1, Pallas kernels: none -> 98.3 us  [stationary(): pl.pallas_call(functools.partial(layer_kernel, n, nt, group), out_shape=j...]
    all_gather x6 -> x0, blocking collectives: 92.5 us -> none  [the longest x2 25.2 us: entering(): lax.all_gather(part.astype(kind), axis)]
    all_gather x6 -> x0, waiting for transfers between devices: 44.6 us -> none  [the longest x1 27.1 us: on_device(): lax.all_gather(rec_i_weight, 'sp', axis=1, tiled=True)]
    dot_general x18 -> x0, matrix products: 28.4 us -> none  [the longest x2 13.3 us: block_pass(): jnp.einsum('thk,tshk,shk->ths', query_rows, decay, keyed_values, precisio...]
    reduce_scatter x1 -> x0, waiting for transfers between devices: 21.2 us -> none  [on_device(): lax.psum_scatter((jnp.dot(att_out, att_rows, preferred_element_type=jnp.f...]
    dot_general x2 -> x0, other arithmetic: 11.8 us -> none  [block_pass(): jnp.einsum('thk,tshk,shk->ths', query_rows, decay, keyed_values, precisio...]
    another operation x7 -> x0, other arithmetic: 6.13 us -> none
    unnamed x7 -> x0, waiting for transfers between devices: 3.68 us -> none
  transfers between devices with their start and end apart: 7 -> 0, of which waited for: 3 -> 0; matrix products, arithmetic and copies ran while one was open for 22% -> 0% of each run, Pallas kernels for 0% -> 0%
where the time goes in v2:
time: 101 us; the launch traced here: 99.9 us
  Pallas kernels  98.3 us (97%)
  local copies, waits for them, and re-layouts  1.57 us (2%)
    pallas_call x1, Pallas kernels, stationary(): pl.pallas_call(functools.partial(layer_kernel, n, nt, group), out_shape=j...  98.3 us

profile of v2, /device:TPU:0, one launch (start us, length us, event | category | flops | bytes accessed | tf_op | source)
XLA Modules:
  0.0 99.9 jit_solution(12484225103264544023)
XLA Ops:
  0.0 98.3 %layer.1 = bf16[32,2048]{1,0:T(8,128)(2,1)} custom-call(bf16[128,512]{1,0:T(8,128)(2,1)} %tok_ref.1, f32[1,2048]{1,0:T(1,128)} %bitcast.3, bf16[256,512]{1,0:T(8,128)(2,1)} %aq_ref.1, bf16[128,512]{1,0:T(8,128)(2,1)} %ak_ref.1, bf16[128,512]{1,0:T(8,128)(2,1)} %av_ref.1, bf16[256,512]{1,0:T(8,128)(2,1)} %rq_ref.1, bf16[256,512]{1,0:T(8,128)(2,1)} %rf_ref.1, ...), custom_call_target="tpu_custom_call" | custom-call | tf_op jit(solution)/shard_map/layer/pallas_call | solution.py:661
  98.3 1.6 %copy.16 = bf16[32,2048]{1,0:T(8,128)(2,1)} copy(bf16[32,2048]{1,0:T(8,128)(2,1)} %layer.1) | data formatting | bytes 262144

commit v3 on v2

--- a/solution.py
+++ b/solution.py
@@ -260,7 +260,8 @@
     )
 
 
-SUB = 64
+SUB = 32
+LAG = 3.5
 
 
 def stick_block(q, j, group, x, offset_ref):
@@ -402,10 +403,6 @@
             shift_ref.at[:, pl.ds(i * REC_KEY, REC_KEY)], shifts.at[pl.ds(s * rows, rows)], d_local
         )
 
-    for i, u in enumerate(ends):
-        pl.when(s != u)(lambda i=i: shift_copy(i).start())
-        pl.when(s == u)(lambda i=i: shift_here(i).start())
-
     def second_copy(k, d):
         return remote(
             tbuf.at[k, t], tbuf.at[k, t], b_send.at[k, d], b_recv.at[k, d],
@@ -476,14 +473,11 @@
         for i in range(2):
             pl.when(s != ends[i])(lambda i=i: square_copy(k, i).start())
 
-    def forward(k):
-        for r in range(subs):
-            c = k * subs + r
-            for i in (1, 0):
-                chain_copy(i, c).wait_recv()
-                at = (i, pl.ds(c * SUB, SUB))
-                sent[at] = (part[at] + came[at].astype(f32)).astype(bf16)
-                chain_copy(i, c).start()
+    def forward(i, c):
+        chain_copy(i, c).wait_recv()
+        at = (i, pl.ds(c * SUB, SUB))
+        sent[at] = (part[at] + came[at].astype(f32)).astype(bf16)
+        chain_copy(i, c).start()
 
     def head_copy(i, k, to):
         at = (i, pl.ds(k * rows, rows))
@@ -571,11 +565,19 @@
         if k + 1 < n:
             relay(k + 1)
         project(k)
-
-    @pl.when(jnp.logical_not(at_end))
-    def _():
-        for k in range(n):
-            forward(k)
+        if k == 0:
+            for i, u in enumerate(ends):
+                pl.when(s != u)(lambda i=i: shift_copy(i).start())
+                pl.when(s == u)(lambda i=i: shift_here(i).start())
+
+    for v in range(1, n - 1):
+        events = [(c + LAG * v, 1, c) for c in range(n * subs)]
+        events += [(c + LAG * (n - 1 - v), 0, c) for c in range(n * subs)]
+
+        @pl.when(s == v)
+        def _():
+            for _, i, c in sorted(events):
+                forward(i, c)
 
     @pl.when(at_end)
     def _():

time: 101 us -> 64.7 us (0.64)
  Pallas kernels: 98.3 us -> 62.5 us
    pallas_call x1, Pallas kernels: 98.3 us -> 62.5 us  [stationary(): pl.pallas_call(functools.partial(layer_kernel, n, nt, group), out_shape=j...]
where the time goes in v3:
time: 64.7 us; the launch traced here: 64.1 us
  Pallas kernels  62.5 us (97%)
  local copies, waits for them, and re-layouts  1.57 us (2%)
    pallas_call x1, Pallas kernels, stationary(): pl.pallas_call(functools.partial(layer_kernel, n, nt, group), out_shape=j...  62.5 us
    unnamed x1, local copies, waits for them, and re-layouts  1.57 us

profile of v3, /device:TPU:0, one launch (start us, length us, event | category | flops | bytes accessed | tf_op | source)
XLA Modules:
  0.0 64.1 jit_solution(18160280621494979110)
XLA Ops:
  0.0 62.5 %layer.1 = bf16[32,2048]{1,0:T(8,128)(2,1)} custom-call(bf16[128,512]{1,0:T(8,128)(2,1)} %tok_ref.1, f32[1,2048]{1,0:T(1,128)} %bitcast.3, bf16[256,512]{1,0:T(8,128)(2,1)} %aq_ref.1, bf16[128,512]{1,0:T(8,128)(2,1)} %ak_ref.1, bf16[128,512]{1,0:T(8,128)(2,1)} %av_ref.1, bf16[256,512]{1,0:T(8,128)(2,1)} %rq_ref.1, bf16[256,512]{1,0:T(8,128)(2,1)} %rf_ref.1, ...), custom_call_target="tpu_custom_call" | custom-call | tf_op jit(solution)/shard_map/layer/pallas_call | solution.py:663
  62.5 1.6 %copy.16 = bf16[32,2048]{1,0:T(8,128)(2,1)} copy(bf16[32,2048]{1,0:T(8,128)(2,1)} %layer.1) | data formatting | bytes 262144
